TPU v7x, 256 devices: a whole 4x4x8 slice. The times are simulated.
256 devices in a mesh: ep: 64 (over z, x, core), tp: 4 (over y).
Axes of the slice: x: 4, y: 4, z: 8, core: 2. Of those that a mesh axis runs over, the one named last changes fastest.
Arguments:
- query_rows: bfloat16 [8192, 1024], P('ep', 'tp'), may hold values from -6 to 6
- key_rows: bfloat16 [8192, 256], P('ep', 'tp'), may hold values from -6 to 6
- retrieved_vector_table: bfloat16 [8192, 256], P('ep', 'tp'), may hold values from -6 to 6
- key_bias: bfloat16 [8192, 4], P('ep', 'tp'), may hold values from -1.5 to 12
- score_offset: float32 [16], P('tp'), may hold values from 3 to 12
- out_weight: bfloat16 [1024, 2048], P('tp'), may hold values from -0.1875 to 0.1875
- second_batch_activations: bfloat16 [8192, 2048], P('ep'), may hold values from -6 to 6
- norm_gain: float32 [2048], replicated, may hold values from 0.1 to 1.9
- expert_index: int32 [8192, 2], P('ep'), may hold values from 0 to 63, all different within a row; in each aligned block of 128 rows (0 to 127, 128 to 255, ...) at most 8 rows name the same one
- route_weight: float32 [8192, 2], P('ep'), may hold values from 0.2 to 1
- gate_weight: bfloat16 [64, 2048, 1024], P('ep', None, 'tp'), may hold values from -0.125 to 0.125
- up_weight: bfloat16 [64, 2048, 1024], P('ep', None, 'tp'), may hold values from -0.125 to 0.125
- down_weight: bfloat16 [64, 1024, 2048], P('ep', 'tp'), may hold values from -0.1875 to 0.1875
Outputs:
- attention_out: bfloat16 [8192, 2048], P(('ep', 'tp'))
- expert_out: bfloat16 [8192, 2048], P('ep', 'tp')
Inputs may be any that keep to these rules, and one draw needn't show every extreme that they name: `expert_index`: each row names 2 different experts; in each aligned block of 128 rows (the rows of one index of ep) no expert is named by more than 8 rows, a bound that some block reaches.
All inputs are finite; a program needn't handle non-finite values.
Results may differ from a plain program's by a relative error of at most 0.011.
Values may be sent and summed in bfloat16 or wider, within the bound.
A program may use at most 64 MiB of HBM per device.

v0:
```python
import math

import jax
import jax.numpy as jnp
from jax import lax
from jax.sharding import PartitionSpec as P

HD = 64
SEQS = 1


def passed_along(array, axis, by):
    peers = lax.axis_size(axis)
    pairs = [(i, i + by) for i in range(peers) if 0 <= i + by < peers]
    return lax.ppermute(array, axis, pairs)


def block_terms(query_block, key_block, value_block, bias_block, offset, causal_mask):
    scale = 1.0 / math.sqrt(query_block.shape[-1])
    scores = (
        jnp.einsum("tkgd,skd->kgts", query_block, key_block, preferred_element_type=jnp.float32)
        * scale
    )
    scores = (
        scores
        + jnp.transpose(bias_block.astype(jnp.float32))[:, None, None, :]
        - offset[:, :, None, None]
    )
    length = query_block.shape[0]
    if causal_mask:
        later = lax.broadcasted_iota(jnp.int32, (length, length), 0) > lax.broadcasted_iota(
            jnp.int32, (length, length), 1
        )
        keep = jnp.where(later, jax.nn.log_sigmoid(-scores), 0.0)
        suffix = lax.cumsum(keep, axis=3, reverse=True) - keep
        weight = jnp.where(later, jnp.exp(jax.nn.log_sigmoid(scores) + suffix), 0.0)
    else:
        keep = jax.nn.log_sigmoid(-scores)
        suffix = lax.cumsum(keep, axis=3, reverse=True) - keep
        weight = jnp.exp(jax.nn.log_sigmoid(scores) + suffix)
    weight = weight.astype(jnp.bfloat16)
    block_out = jnp.einsum(
        "kgts,skd->kgtd", weight, value_block, preferred_element_type=jnp.float32
    )
    return (block_out, jnp.sum(keep, axis=3))


def attention_half(
    query_rows, key_rows, retrieved_vector_table, key_bias, score_offset, out_weight
):
    length = query_rows.shape[0]
    kv_local = key_rows.shape[1] // HD
    group = query_rows.shape[1] // HD // kv_local
    query_block = query_rows.reshape(length, kv_local, group, HD)
    key_block = key_rows.reshape(length, kv_local, HD)
    value_block = retrieved_vector_table.reshape(length, kv_local, HD)
    offset = score_offset.reshape(kv_local, group)
    span = lax.axis_size("ep") // SEQS
    sequence_place_index = lax.axis_index("ep") % span
    result, near = block_terms(query_block, key_block, value_block, key_bias, offset, True)

    def step(distance, state):
        result, near, moving = state
        moving = passed_along((moving[0], moving[1], moving[2]), "ep", 1)
        block_out, total = block_terms(query_block, moving[0], moving[1], moving[2], offset, False)
        valid = sequence_place_index >= distance
        result = jnp.where(valid, result + jnp.exp(near)[..., None] * block_out, result)
        near = jnp.where(valid, near + total, near)
        return (result, near, moving)

    result, near, moving = lax.fori_loop(
        1, span, step, (result, near, (key_block, value_block, key_bias))
    )
    attended = (
        jnp.transpose(result, (2, 0, 1, 3))
        .reshape(length, kv_local * group * HD)
        .astype(jnp.bfloat16)
    )
    return lax.psum_scatter(
        jnp.dot(attended, out_weight, preferred_element_type=jnp.float32).astype(jnp.bfloat16),
        "tp",
        scatter_dimension=0,
        tiled=True,
    )


def expert_half(
    second_batch_activations,
    norm_gain,
    expert_index,
    route_weight,
    gate_weight,
    up_weight,
    down_weight,
):
    tokens = second_batch_activations.shape[0]
    picks = expert_index.shape[1]
    experts = lax.axis_size("ep")
    capacity = 2 * tokens * picks // experts
    values32 = second_batch_activations.astype(jnp.float32)
    normed = (
        values32
        * lax.rsqrt(jnp.mean(values32 * values32, axis=1, keepdims=True) + 1e-06)
        * norm_gain
    ).astype(jnp.bfloat16)
    flat = expert_index.reshape(-1)
    indicator_matrix = (flat[:, None] == jnp.arange(experts, dtype=jnp.int32)[None, :]).astype(
        jnp.int32
    )
    slot = jnp.sum(indicator_matrix * (jnp.cumsum(indicator_matrix, axis=0) - 1), axis=1)
    target = flat * capacity + slot
    source_row = (
        jnp.full((experts * capacity,), tokens, jnp.int32)
        .at[target]
        .set(jnp.arange(flat.shape[0], dtype=jnp.int32) // picks)
    )
    padded = jnp.concatenate([normed, jnp.zeros((1, normed.shape[1]), jnp.bfloat16)], axis=0)
    outgoing = padded[source_row].reshape(experts, capacity, padded.shape[1])
    gate_local = gate_weight[0]
    up_local = up_weight[0]
    down_local = down_weight[0]
    arrived = lax.all_to_all(outgoing, "ep", split_axis=0, concat_axis=0, tiled=True)
    gate_pre = jnp.einsum("scd,df->scf", arrived, gate_local, preferred_element_type=jnp.float32)
    up_pre = jnp.einsum("scd,df->scf", arrived, up_local, preferred_element_type=jnp.float32)
    hidden = (jax.nn.silu(gate_pre) * up_pre).astype(jnp.bfloat16)
    partial_value = jnp.einsum(
        "scf,fd->scd", hidden, down_local, preferred_element_type=jnp.float32
    )
    summed = lax.psum_scatter(
        partial_value.astype(jnp.bfloat16), "tp", scatter_dimension=2, tiled=True
    )
    returned = lax.all_to_all(summed, "ep", split_axis=0, concat_axis=0, tiled=True)
    picked = returned.reshape(experts * capacity, returned.shape[2])[target].reshape(
        tokens, picks, returned.shape[2]
    )
    return jnp.sum(route_weight[:, :, None] * picked.astype(jnp.float32), axis=1).astype(
        jnp.bfloat16
    )


def body(
    query_rows,
    key_rows,
    retrieved_vector_table,
    key_bias,
    score_offset,
    out_weight,
    second_batch_activations,
    norm_gain,
    expert_index,
    route_weight,
    gate_weight,
    up_weight,
    down_weight,
):
    attention_out = attention_half(
        query_rows, key_rows, retrieved_vector_table, key_bias, score_offset, out_weight
    )
    expert_out = expert_half(
        second_batch_activations,
        norm_gain,
        expert_index,
        route_weight,
        gate_weight,
        up_weight,
        down_weight,
    )
    return (attention_out, expert_out)


def solution(mesh):
    return jax.shard_map(
        body,
        mesh=mesh,
        in_specs=(
            P("ep", "tp"),
            P("ep", "tp"),
            P("ep", "tp"),
            P("ep", "tp"),
            P("tp"),
            P("tp", None),
            P("ep", None),
            P(),
            P("ep", None),
            P("ep", None),
            P("ep", None, "tp"),
            P("ep", None, "tp"),
            P("ep", "tp", None),
        ),
        out_specs=(P(("ep", "tp"), None), P("ep", "tp")),
        check_vma=False,
    )
```

profile of v0, /device:TPU:1, one launch (start us, length us, event | category | flops | bytes accessed | tf_op | source)
XLA Modules:
  0.0 1108.2 jit_solution(7254555710618742797)
XLA Ops:
  19.7 13.1 %all-to-all-start = ((bf16[64,8,2048]{2,1,0:T(8,128)(2,1)}), bf16[64,8,2048]{2,1,0:T(8,128)(2,1)S(1)}, u32[]{:S(2)}, u32[]{:S(2)}) async-start(bf16[64,8,2048]{2,1,0:T(8,128)(2,1)} %bitcast.127), calls=%async_computation.1 | async-start | bytes 4194304 | tf_op jit(solution)/shard_map/all_to_all | solution.py:122
  34.3 5.1 reduce_window_sum.33
  40.9 41.6 %all-to-all-done = bf16[64,8,2048]{2,1,0:T(8,128)(2,1)S(1)} async-done(((bf16[64,8,2048]{2,1,0:T(8,128)(2,1)}), bf16[64,8,2048]{2,1,0:T(8,128)(2,1)S(1)}, u32[]{:S(2)}, u32[]{:S(2)}) %all-to-all-start) | async-done | bytes 2097184 | tf_op jit(solution)/shard_map/all_to_all | solution.py:122
  85.2 5.0 convolution_convert_fusion
  90.3 956.9 %while.21 = (s32[]{:T(128)}, f32[1,4,128,64]{2,3,1,0:T(8,128)S(1)}, f32[1,4,128]{2,1,0:T(4,128)S(1)}, bf16[128,1,64]{0,2,1:T(8,128)(2,1)S(1)}, bf16[128,1,64]{0,...) while((s32[]{:T(128)}, f32[1,4,128,64]{2,3,1,0:T(8,128)S(1)}, ...), condition=%wide.region_5.6_spmd, body=%wide.region_2.5_spmd.sunk | while | flops 27100288 | bytes 2145284 | solution.py:71
  90.5 5.2 collective-permute-start.1
  462.5 4.7 collective-permute-start.2
  478.0 4.7 collective-permute-start.2
  493.6 4.7 collective-permute-start.2
  509.1 4.7 collective-permute-start.2
  524.6 4.7 collective-permute-start.2
  540.1 4.7 collective-permute-start.2
  555.7 4.7 collective-permute-start.2
  571.2 4.7 collective-permute-start.2
  757.5 4.7 collective-permute-start.2
  773.1 4.7 collective-permute-start.2
  788.6 4.7 collective-permute-start.2
  804.1 4.7 collective-permute-start.2
  819.6 4.7 collective-permute-start.2
  835.2 4.7 collective-permute-start.2
  850.7 4.7 collective-permute-start.2
  1047.2 27.2 %all-to-all-start.1 = ((bf16[64,8,512]{2,1,0:T(8,128)(2,1)}), bf16[64,8,512]{2,1,0:T(8,128)(2,1)S(1)}, u32[]{:S(2)}, u32[]{:S(2)}) async-start(bf16[64,8,512]{2,1,0:T(8,128)(2,1)} %reduce-scatter.5.cloned.1.call-done), calls=%async_computation.3 | async-start | bytes 1048576 | tf_op jit(solution)/shard_map/all_to_all | solution.py:132
  1075.8 16.3 %all-to-all-done.1 = bf16[64,8,512]{2,1,0:T(8,128)(2,1)S(1)} async-done(((bf16[64,8,512]{2,1,0:T(8,128)(2,1)}), bf16[64,8,512]{2,1,0:T(8,128)(2,1)S(1)}, u32[]{:S(2)}, u32[]{:S(2)}) %all-to-all-start.1) | async-done | bytes 524320 | tf_op jit(solution)/shard_map/all_to_all | solution.py:132
  1095.0 6.4 reduce-scatter.3.cloned.1.call-done
  (919 shorter events, 896.6 us)
Async XLA Ops:
  19.7 62.8 %all-to-all-start = ((bf16[64,8,2048]{2,1,0:T(8,128)(2,1)}), bf16[64,8,2048]{2,1,0:T(8,128)(2,1)S(1)}, u32[]{:S(2)}, u32[]{:S(2)}) async-start(bf16[64,8,2048]{2,1,0:T(8,128)(2,1)} %bitcast.127), calls=%async_computation.1 | async-start | bytes 4194304 | tf_op jit(solution)/shard_map/all_to_all | solution.py:122
  32.8 1014.5 %reduce-scatter.5.cloned.1.call-start = ((), (), s32[]{:S(2)}) async-start(), calls=%async_computation.5 | async-start | bytes 2621440 | tf_op jit(solution)/shard_map/reduce_scatter | solution.py:129
  90.5 10.7 collective-permute-start.1
  332.9 10.1 collective-permute-start.1
  348.4 10.1 collective-permute-start.1
  363.9 10.1 collective-permute-start.1
  379.4 10.1 collective-permute-start.1
  395.0 10.1 collective-permute-start.1
  410.5 10.1 collective-permute-start.1
  426.0 10.1 collective-permute-start.1
  441.6 10.1 collective-permute-start.1
  457.1 10.1 collective-permute-start.1
  472.6 10.1 collective-permute-start.1
  488.1 10.1 collective-permute-start.1
  503.7 10.1 collective-permute-start.1
  519.2 10.1 collective-permute-start.1
  534.7 10.1 collective-permute-start.1
  550.3 10.1 collective-permute-start.1
  565.8 10.1 collective-permute-start.1
  581.3 10.1 collective-permute-start.1
  596.8 10.1 collective-permute-start.1
  612.4 10.1 collective-permute-start.1
  1047.2 44.9 %all-to-all-start.1 = ((bf16[64,8,512]{2,1,0:T(8,128)(2,1)}), bf16[64,8,512]{2,1,0:T(8,128)(2,1)S(1)}, u32[]{:S(2)}, u32[]{:S(2)}) async-start(bf16[64,8,512]{2,1,0:T(8,128)(2,1)} %reduce-scatter.5.cloned.1.call-done), calls=%async_computation.3 | async-start | bytes 1048576 | tf_op jit(solution)/shard_map/all_to_all | solution.py:132
  1074.4 27.0 %reduce-scatter.3.cloned.1.call-start = ((), (), s32[]{:S(2)}) async-start(), calls=%async_computation.4 | async-start | bytes 655360 | tf_op jit(solution)/shard_map/reduce_scatter | solution.py:79
  (174 other events, 2509.8 us)
Sparse Core Ops, SparseCore 0:
  90.4 29.9 reduce-scatter.4
  1078.3 22.9 reduce-scatter.2
where the time goes:
time: 1120 us; the launch traced here: 1110 us
  starting transfers between devices  654 us (58%)
  other arithmetic  291 us (26%)
  matrix products  67 us (6%)
  waiting for transfers between devices  64.9 us (6%)
  between operations  14.3 us (1%)
    ppermute x189, starting transfers between devices, passed_along(): return lax.ppermute(array, axis, pairs)  613 us
    another operation x64, other arithmetic, block_terms(): suffix = lax.cumsum(keep, axis=3, reverse=True) - keep  284 us
    all_to_all x1, waiting for transfers between devices, expert_half(): lax.all_to_all(outgoing, 'ep', split_axis=0, concat_axis=0, tiled=True)  41.6 us
    dot_general x64, matrix products, block_terms(): jnp.einsum('kgts,skd->kgtd', weight, value_block, preferred_element_type=...  33.4 us
    all_to_all x1, starting transfers between devices, expert_half(): lax.all_to_all(summed, 'ep', split_axis=0, concat_axis=0, tiled=True)  27.2 us
    dot_general x64, matrix products, block_terms(): jnp.einsum('tkgd,skd->kgts', query_block, key_block, preferred_element_ty...  24.7 us
  transfers between devices with their start and end apart: 193, of which 3 were waited for; matrix products, arithmetic and copies ran while one was open for 31% of the time, Pallas kernels for 0%

commit v1 on v0

v1 whole, which is shorter than its diff:
```python
import jax
import jax.numpy as jnp
from jax import lax
from jax.experimental import pallas as pl
from jax.experimental.pallas import tpu as pltpu
from jax.sharding import PartitionSpec as P

HD = 64
LOG2E = 1.4426950408889634
ROWS = 128


def block_update(lhs, off, kv, bias_row, tri, near, diag):
    rhs = jnp.concatenate([kv, kv], axis=1)
    dot = lax.dot_general(lhs, rhs, (((1,), (1,)), ((), ())), preferred_element_type=jnp.float32)
    heads = dot.shape[0] // ROWS
    s = jnp.concatenate(
        [dot[h * ROWS : (h + 1) * ROWS] + (bias_row - off[h]) for h in range(heads)], axis=0
    )
    small = jnp.log2(1.0 + jnp.exp2(-jnp.abs(s)))
    soft = jnp.maximum(s, 0.0) + small
    logw = jnp.minimum(s, 0.0) - small
    if diag:
        row = lax.broadcasted_iota(jnp.int32, s.shape, 0) % ROWS
        later = row > lax.broadcasted_iota(jnp.int32, s.shape, 1)
        soft = jnp.where(later, soft, 0.0)
    sums = jnp.dot(soft.astype(jnp.bfloat16), tri, preferred_element_type=jnp.float32)
    expo = logw - sums[:, :ROWS]
    if near is not None:
        expo = expo - near
    w = jnp.exp2(expo)
    if diag:
        w = jnp.where(later, w, 0.0)
    out = jnp.dot(w.astype(jnp.bfloat16), kv, preferred_element_type=jnp.float32)
    return out, sums[:, ROWS:]


def query_lhs(q):
    q2 = q.astype(jnp.float32) * (0.125 * LOG2E)
    hi = q2.astype(jnp.bfloat16)
    lo = (q2 - hi.astype(jnp.float32)).astype(jnp.bfloat16)
    zero = jnp.zeros((ROWS, HD), jnp.bfloat16)
    parts = []
    for h in range(q.shape[1] // HD):
        cut = slice(h * HD, (h + 1) * HD)
        parts.append(jnp.concatenate([hi[:, cut], zero, lo[:, cut], zero], axis=1))
    return jnp.concatenate(parts, axis=0)


def triangle():
    r = lax.broadcasted_iota(jnp.int32, (ROWS, 2 * ROWS), 0)
    c = lax.broadcasted_iota(jnp.int32, (ROWS, 2 * ROWS), 1)
    return jnp.where((r > c) | (c >= ROWS), 1.0, 0.0).astype(jnp.bfloat16)


NX, NC, CAP = 4, 2, 8
DISTANCES = ((0, 1), (7, 2), (6, 3), (5, 4))
MESH = pl.DeviceIdType.MESH


def whole_kernel(
    off_ref, pack_ref, q_ref, act_ref, gain_ref, idx_ref, idxt_ref, route_ref, wg_hbm, wu_hbm, wd_hbm, wo_hbm,
    att_out, exp_out,
    kvb, lhs_ref, tri_ref, acc_ref, near_ref,
    wg, wu, wd, wo,
    outgoing, pick, arr, part, rs1l, rs1r, rs2l, rs2r, res, ret,
    apart, ars1l, ars1r, ars2l, ars2r,
    wsem, lsem, kzs, kzr, kxs, kxr, kcs, kcr, ds, dr, ags, agr, rss, rsr, rts, rtr, ats, atr,
):
    e, t = lax.axis_index("ep"), lax.axis_index("tp")
    nz = lax.axis_size("ep") // (NX * NC)
    ne = nz * NX * NC
    tokens = act_ref.shape[0]
    heads = q_ref.shape[1] // HD
    groups = arr.shape[1]
    wide = arr.shape[-1]
    z, x, c = e // (NX * NC), e // NC % NX, e % NC
    xc = x * NC + c
    left, right, opp = (t + 3) % 4, (t + 1) % 4, (t + 2) % 4

    def ep_of(z_, x_, c_):
        return (z_ * NX + x_) * NC + c_

    def rc(src, dst, ssem, rsem, dev):
        return pltpu.make_async_remote_copy(
            src_ref=src, dst_ref=dst, send_sem=ssem, recv_sem=rsem, device_id=dev, device_id_type=MESH
        )

    barrier = pltpu.get_barrier_semaphore()

    def greet(i, carry):
        pl.semaphore_signal(barrier, inc=1, device_id=((e + i) % ne, t), device_id_type=MESH)
        return carry

    lax.fori_loop(1, ne, greet, 0)
    for near_t in (left, right):
        pl.semaphore_signal(barrier, inc=1, device_id=(e, near_t), device_id_type=MESH)

    loads = [
        pltpu.make_async_copy(src, dst, wsem.at[i])
        for i, (src, dst) in enumerate(((wg_hbm, wg), (wu_hbm, wu), (wd_hbm, wd), (wo_hbm, wo)))
    ]
    for load in loads:
        load.start()
    own_kv = pltpu.make_async_copy(pack_ref, kvb.at[xc, z], lsem.at[0])
    own_kv.start()

    values = act_ref[...].astype(jnp.float32)
    inv = lax.rsqrt(jnp.mean(values * values, axis=1, keepdims=True) + 1e-06)
    mine = pl.ds(pl.multiple_of(t * wide, wide), wide)
    normed = (act_ref[:, mine].astype(jnp.float32) * inv * gain_ref[:, mine]).astype(jnp.bfloat16)
    i0 = lax.broadcasted_iota(jnp.int32, (tokens, tokens), 0)
    i1 = lax.broadcasted_iota(jnp.int32, (tokens, tokens), 1)
    below = jnp.where(i0 > i1, 1.0, 0.0).astype(jnp.bfloat16)
    above = jnp.where(i0 < i1, 1.0, 0.0).astype(jnp.bfloat16)
    eq = [jnp.where(i1 == idx_ref[:, k : k + 1], 1.0, 0.0) for k in range(2)]
    prefix = jnp.dot(below, (eq[0] + eq[1]).astype(jnp.bfloat16), preferred_element_type=jnp.float32)
    eqt = [jnp.where(i0 == idxt_ref[k : k + 1, :], 1.0, 0.0) for k in range(2)]
    prefixt = jnp.dot((eqt[0] + eqt[1]).astype(jnp.bfloat16), above, preferred_element_type=jnp.float32)
    slots = ne * CAP
    col = lax.broadcasted_iota(jnp.int32, (tokens, slots), 1).astype(jnp.float32)
    row = lax.broadcasted_iota(jnp.int32, (slots, tokens), 0).astype(jnp.float32)
    spread = None
    for k in range(2):
        place = jnp.sum(eq[k] * prefix, axis=1, keepdims=True) + idx_ref[:, k : k + 1].astype(jnp.float32) * CAP
        pick[k] = jnp.where(col == place, 1.0, 0.0).astype(jnp.bfloat16)
        placet = jnp.sum(eqt[k] * prefixt, axis=0, keepdims=True) + idxt_ref[k : k + 1, :].astype(jnp.float32) * CAP
        one = jnp.where(row == placet, 1.0, 0.0)
        spread = one if spread is None else spread + one
    sent = jnp.dot(spread.astype(jnp.bfloat16), normed, preferred_element_type=jnp.float32)
    outgoing[...] = sent.reshape(ne, CAP, wide).astype(jnp.bfloat16)
    lhs_ref[...] = query_lhs(q_ref[...])
    tri_ref[...] = triangle()
    off = [off_ref[h] * LOG2E for h in range(heads)]

    pl.semaphore_wait(barrier, ne + 1)

    def to_z(i, carry):
        rc(pack_ref, kvb.at[xc, z], kzs, kzr, (ep_of((z + i) % nz, x, c), t)).start()
        return carry

    lax.fori_loop(1, nz, to_z, 0)

    def peer(g, i, sign):
        per = NX * NC
        dz = jnp.where(i < per, DISTANCES[g][0] % nz, DISTANCES[g][1] % nz)
        dx, dc = i // NC % NX, i % NC
        if sign < 0:
            dz, dx = nz - dz, NX - dx
        return ep_of((z + dz) % nz, (x + dx) % NX, (c + dc) % NC)

    own_rows = pltpu.make_async_copy(outgoing.at[e], arr.at[t, 0, 0], lsem.at[1])
    own_rows.start()
    for g in range(groups):

        def scatter(i, carry, g=g):
            to = peer(g, i, 1)
            rc(outgoing.at[to], arr.at[t, g, i], ds.at[g], dr.at[g], (to, t)).start()
            return carry

        lax.fori_loop(1 if g == 0 else 0, 2 * NX * NC, scatter, 0)

    def arrived(g):
        ref = arr.at[t, g, 1:] if g == 0 else arr.at[t, g]
        return rc(ref, ref, ds.at[g], dr.at[g], (e, t))

    half = arr.shape[2] // 2
    at_right, at_left = (e, right), (e, left)

    def ag(g):
        return [
            rc(arr.at[t, g], arr.at[t, g], ags.at[0, g], agr.at[0, g], at_right),
            rc(arr.at[t, g], arr.at[t, g], ags.at[1, g], agr.at[1, g], at_left),
            rc(arr.at[left, g, :half], arr.at[left, g, :half], ags.at[2, g], agr.at[2, g], at_right),
            rc(arr.at[right, g, half:], arr.at[right, g, half:], ags.at[3, g], agr.at[3, g], at_left),
        ]

    ags_all = [ag(g) for g in range(groups)]

    def spread_rows(g):
        arrived(g).wait_recv()
        if g == 0:
            own_rows.wait()
        ags_all[g][0].start()
        ags_all[g][1].start()

    def forward_rows(g):
        ags_all[g][0].wait_recv()
        ags_all[g][2].start()
        ags_all[g][1].wait_recv()
        ags_all[g][3].start()

    xl, xr, xo = (x + 3) % NX, (x + 1) % NX, (x + 2) % NX
    dev_xr, dev_xl, dev_c = (ep_of(z, xr, c), t), (ep_of(z, xl, c), t), (ep_of(z, x, (c + 1) % NC), t)
    zh = nz // 2

    def grp(x_):
        return kvb.at[x_ * NC + c]

    kx = [
        rc(grp(x), grp(x), kxs.at[0], kxr.at[0], dev_xr),
        rc(grp(x), grp(x), kxs.at[1], kxr.at[1], dev_xl),
        rc(kvb.at[xl * NC + c, :zh], kvb.at[xl * NC + c, :zh], kxs.at[2], kxr.at[2], dev_xr),
        rc(kvb.at[xr * NC + c, zh:], kvb.at[xr * NC + c, zh:], kxs.at[3], kxr.at[3], dev_xl),
    ]
    kc = [rc(grp(x_), grp(x_), kcs.at[i], kcr.at[i], dev_c) for i, x_ in enumerate((x, xl, xr, xo))]
    z_all = rc(kvb.at[xc, 1:], kvb.at[xc, 1:], kzs, kzr, (e, t))

    def kv_first():
        z_all.wait_recv()
        own_kv.wait()
        kx[0].start()
        kx[1].start()
        kc[0].start()

    def kv_second():
        kx[0].wait_recv()
        kx[2].start()
        kc[1].start()
        kx[1].wait_recv()
        kx[3].start()
        kc[2].start()

    def kv_third():
        kx[2].wait_recv()
        kx[3].wait_recv()
        kc[3].start()

    def kv_ready():
        for copy in kc:
            copy.wait_recv()

    rows = arr.shape[2] * CAP

    def flat(ref):
        v = ref[...].astype(jnp.float32)
        return v.reshape(v.shape[0] * v.shape[1], v.shape[2])

    def experts(g):
        ags_all[g][2].wait_recv()
        ags_all[g][3].wait_recv()
        gate = jnp.zeros((rows, wg.shape[1]), jnp.float32)
        up = jnp.zeros((rows, wg.shape[1]), jnp.float32)
        for s in range(4):
            xs = flat(arr.at[s, g]).astype(jnp.bfloat16)
            gate += jnp.dot(xs, wg[s * wide : (s + 1) * wide, :], preferred_element_type=jnp.float32)
            up += jnp.dot(xs, wu[s * wide : (s + 1) * wide, :], preferred_element_type=jnp.float32)
        hidden = (gate / (1.0 + jnp.exp(-gate)) * up).astype(jnp.bfloat16)
        for s in range(4):
            value = jnp.dot(hidden, wd[:, s * wide : (s + 1) * wide], preferred_element_type=jnp.float32)
            part[s, g] = value.reshape(arr.shape[2], CAP, wide).astype(jnp.bfloat16)

    def rs(g):
        return [
            rc(part.at[opp, g, :half], rs1l.at[g], rss.at[0, g], rsr.at[0, g], at_right),
            rc(part.at[opp, g, half:], rs1r.at[g], rss.at[1, g], rsr.at[1, g], at_left),
            rc(part.at[right, g], rs2l.at[g], rss.at[2, g], rsr.at[2, g], at_right),
            rc(part.at[left, g], rs2r.at[g], rss.at[3, g], rsr.at[3, g], at_left),
        ]

    rs_all = [rs(g) for g in range(groups)]

    def add_to(dst, value):
        dst[...] = (dst[...].astype(jnp.float32) + value[...].astype(jnp.float32)).astype(jnp.bfloat16)

    def reduce_first(g):
        rs_all[g][0].start()
        rs_all[g][1].start()

    def reduce_second(g):
        rs_all[g][0].wait_recv()
        add_to(part.at[right, g, :half], rs1l.at[g])
        rs_all[g][2].start()
        rs_all[g][1].wait_recv()
        add_to(part.at[left, g, half:], rs1r.at[g])
        rs_all[g][3].start()

    own_back = pltpu.make_async_copy(res.at[0, 0], ret.at[e], lsem.at[2])

    def give_back(g):
        rs_all[g][2].wait_recv()
        rs_all[g][3].wait_recv()
        total = part[t, g].astype(jnp.float32) + rs2l[g].astype(jnp.float32) + rs2r[g].astype(jnp.float32)
        res[g] = total.astype(jnp.bfloat16)
        if g == 0:
            own_back.start()

        def back(i, carry):
            to = peer(g, i, -1)
            rc(res.at[g, i], ret.at[e], rts.at[g], rtr, (to, t)).start()
            return carry

        lax.fori_loop(1 if g == 0 else 0, 2 * NX * NC, back, 0)

    def block_of(b):
        return b % (NX * NC), b // (NX * NC)

    def load_block(b):
        i, j = block_of(b)
        return kvb[i, j, :ROWS], kvb[i, j, ROWS:][:1].astype(jnp.float32) * LOG2E

    def attend_first():
        kv, bias_row = load_block(e)
        out, total = block_update(lhs_ref[...], off, kv, bias_row, tri_ref[...], None, True)
        acc_ref[...] = out
        near_ref[...] = total

    def attend(piece, pieces):
        def step(i, carry):
            kv, bias_row = load_block(e - i)
            near = near_ref[...]
            out, total = block_update(lhs_ref[...], off, kv, bias_row, tri_ref[...], near, False)
            acc_ref[...] += out
            near_ref[...] = near + total
            return carry

        lax.fori_loop(1 + e * piece // pieces, 1 + e * (piece + 1) // pieces, step, 0)

    aw = apart.shape[1]
    ah = aw // 2
    ar = [
        rc(apart.at[opp, :ah], ars1l, ats.at[0], atr.at[0], at_right),
        rc(apart.at[opp, ah:], ars1r, ats.at[1], atr.at[1], at_left),
        rc(apart.at[right], ars2l, ats.at[2], atr.at[2], at_right),
        rc(apart.at[left], ars2r, ats.at[3], atr.at[3], at_left),
    ]

    def project():
        lane = lax.broadcasted_iota(jnp.int32, (ROWS, ROWS), 1)
        pairs = []
        for h in range(0, heads, 2):
            even = pltpu.roll(acc_ref[h * ROWS : (h + 1) * ROWS, :], HD, 1)
            odd = acc_ref[(h + 1) * ROWS : (h + 2) * ROWS, :]
            pairs.append(jnp.where(lane < HD, even, odd))
        attended = jnp.concatenate(pairs, axis=1).astype(jnp.bfloat16)
        step = 512
        for s in range(0, wo.shape[1], step):
            value = jnp.dot(attended, wo[:, s : s + step], preferred_element_type=jnp.float32)
            apart[:, :, s : s + step] = value.reshape(4, aw, step).astype(jnp.bfloat16)
        ar[0].start()
        ar[1].start()

    def project_second():
        ar[0].wait_recv()
        add_to(apart.at[right, :ah], ars1l)
        ar[2].start()
        ar[1].wait_recv()
        add_to(apart.at[left, ah:], ars1r)
        ar[3].start()

    def project_last():
        ar[2].wait_recv()
        ar[3].wait_recv()
        total = apart[t].astype(jnp.float32) + ars2l[...].astype(jnp.float32) + ars2r[...].astype(jnp.float32)
        att_out[...] = total.astype(jnp.bfloat16)

    spread_rows(0)
    kv_first()
    spread_rows(1)
    for load in loads:
        load.wait()
    forward_rows(0)
    spread_rows(2)
    forward_rows(1)
    spread_rows(3)
    kv_second()
    experts(0)
    reduce_first(0)
    forward_rows(2)
    kv_third()
    forward_rows(3)
    experts(1)
    reduce_first(1)
    reduce_second(0)
    kv_ready()
    attend_first()
    attend(0, 4)
    experts(2)
    reduce_first(2)
    reduce_second(1)
    give_back(0)
    attend(1, 4)
    experts(3)
    reduce_first(3)
    reduce_second(2)
    give_back(1)
    attend(2, 4)
    reduce_second(3)
    give_back(2)
    attend(3, 4)
    project()
    give_back(3)
    project_second()

    all_back = rc(ret.at[1:], ret.at[1:], rts.at[0], rtr, (e, t))
    all_back.wait_recv()
    own_back.wait()
    back_rows = flat(ret).astype(jnp.bfloat16)
    total = None
    for k in range(2):
        got = jnp.dot(pick[k], back_rows, preferred_element_type=jnp.float32) * route_ref[:, k : k + 1]
        total = got if total is None else total + got
    exp_out[...] = total.astype(jnp.bfloat16)
    project_last()

    for g in range(groups):
        arrived(g).wait_send()
        ref = res.at[g, 1:] if g == 0 else res.at[g]
        rc(ref, ref, rts.at[g], rtr, (e, t)).wait_send()
        for copy in ags_all[g] + rs_all[g]:
            copy.wait_send()
    for copy in kx + kc + ar + [z_all]:
        copy.wait_send()


def body(
    query_rows, key_rows, retrieved_vector_table, key_bias, score_offset, out_weight, second_batch_activations,
    norm_gain, expert_index, route_weight, gate_weight, up_weight, down_weight,
):
    ne = lax.axis_size("ep")
    tokens, width = second_batch_activations.shape
    wide = width // 4
    groups = len(DISTANCES)
    each = 2 * NX * NC
    heads = query_rows.shape[1] // HD
    bias_row = jnp.pad(key_bias.reshape(1, ROWS), ((0, 15), (0, 0)))
    pack = jnp.concatenate([jnp.concatenate([key_rows, retrieved_vector_table], axis=1), bias_row], axis=0)
    bf, f32 = jnp.bfloat16, jnp.float32
    vmem, dma = pltpu.VMEM, pltpu.SemaphoreType.DMA
    vspec, aspec = pl.BlockSpec(memory_space=pltpu.VMEM), pl.BlockSpec(memory_space=pl.ANY)
    aw = tokens // 4
    return pl.pallas_call(
        whole_kernel,
        out_shape=(
            jax.ShapeDtypeStruct((aw, width), bf),
            jax.ShapeDtypeStruct((tokens, wide), bf),
        ),
        in_specs=[pl.BlockSpec(memory_space=pltpu.SMEM)] + [vspec] * 7 + [aspec] * 4,
        out_specs=(vspec, vspec),
        scratch_shapes=[
            vmem((NX * NC, ne // (NX * NC), ROWS + 16, ROWS), bf),
            vmem((heads * ROWS, 2 * ROWS), bf),
            vmem((ROWS, 2 * ROWS), bf),
            vmem((heads * ROWS, ROWS), f32),
            vmem((heads * ROWS, ROWS), f32),
            vmem(gate_weight.shape[1:], bf),
            vmem(up_weight.shape[1:], bf),
            vmem(down_weight.shape[1:], bf),
            vmem(out_weight.shape, bf),
            vmem((ne, CAP, wide), bf),
            vmem((2, tokens, ne * CAP), bf),
            vmem((4, groups, each, CAP, wide), bf),
            vmem((4, groups, each, CAP, wide), bf),
            vmem((groups, each // 2, CAP, wide), bf),
            vmem((groups, each // 2, CAP, wide), bf),
            vmem((groups, each, CAP, wide), bf),
            vmem((groups, each, CAP, wide), bf),
            vmem((groups, each, CAP, wide), bf),
            vmem((ne, CAP, wide), bf),
            vmem((4, aw, width), bf),
            vmem((aw // 2, width), bf),
            vmem((aw // 2, width), bf),
            vmem((aw, width), bf),
            vmem((aw, width), bf),
            dma((4,)), dma((3,)), dma, dma, dma((4,)), dma((4,)), dma((4,)), dma((4,)),
            dma((groups,)), dma((groups,)), dma((4, groups)), dma((4, groups)), dma((4, groups)), dma((4, groups)),
            dma((groups,)), dma, dma((4,)), dma((4,)),
        ],
        compiler_params=pltpu.CompilerParams(
            collective_id=0, has_side_effects=True, vmem_limit_bytes=56 * 1024 * 1024
        ),
    )(
        score_offset, pack, query_rows, second_batch_activations, norm_gain.reshape(1, width), expert_index,
        expert_index.T, route_weight, gate_weight[0], up_weight[0], down_weight[0], out_weight,
    )


def solution(mesh):
    return jax.shard_map(
        body,
        mesh=mesh,
        in_specs=(
            P("ep", "tp"),
            P("ep", "tp"),
            P("ep", "tp"),
            P("ep", "tp"),
            P("tp"),
            P("tp", None),
            P("ep", None),
            P(),
            P("ep", None),
            P("ep", None),
            P("ep", None, "tp"),
            P("ep", None, "tp"),
            P("ep", "tp", None),
        ),
        out_specs=(P(("ep", "tp"), None), P("ep", "tp")),
        check_vma=False,
    )
```

time: 1120 us -> 95.1 us (0.08)
  the two profiles are of different devices: /device:TPU:1 before, /device:TPU:64 now
where the time goes in v1:
time: 95.1 us; the launch traced here: 94.9 us
  Pallas kernels  88.3 us (93%)
  local copies, waits for them, and re-layouts  5.23 us (5%)
    pallas_call x1, Pallas kernels, body(): pl.pallas_call(whole_kernel, out_shape=(jax.ShapeDtypeStruct((aw, width),...  88.3 us
    unnamed x16, local copies, waits for them, and re-layouts  5.23 us

profile of v1, /device:TPU:64, one launch (start us, length us, event | category | flops | bytes accessed | tf_op | source)
XLA Modules:
  0.0 94.9 jit_solution(7821185950806124927)
XLA Ops:
  0.6 0.0 copy-start.1
  0.6 0.8 copy.15
  1.5 0.0 copy-done.1
  1.5 0.0 copy-start.4
  1.5 0.1 copy.16
  1.6 0.5 copy-done.4
  2.1 0.0 copy-start.3
  2.1 0.7 fusion.1.pack_ref
  2.8 0.0 copy-done.3
  2.8 0.0 copy-start.2
  2.8 0.7 copy.18.route_ref
  3.6 0.0 copy-done.2
  3.6 0.7 copy.17.idx_ref
  4.3 88.3 %shard_map.140 = (bf16[32,2048]{1,0:T(8,128)(2,1)}, bf16[128,512]{1,0:T(8,128)(2,1)}) custom-call(f32[4]{0:T(128)} %off_ref.1, bf16[144,128]{1,0:T(8,128)(2,1)} %fusion.1.pack_ref, bf16[128,256]{1,0:T(8,128)(2,1)} %q_ref.1, bf16[128,2048]{1,0:T(8,128)(2,1)} %act_ref.1, f32[1,2048]{1,0:T(1,128)} %bitcast.9, s32[128,2]{1,0:T(8,128)} %copy.17.idx_ref, ...), custom_call_target="tpu_custom_call" | custom-call | tf_op jit(solution)/shard_map/pallas_call | solution.py:432
  92.6 0.0 copy-start
  92.6 1.6 %copy.21 = bf16[32,2048]{1,0:T(8,128)(2,1)} copy(bf16[32,2048]{1,0:T(8,128)(2,1)} %get-tuple-element.4) | data formatting | bytes 262144
  94.2 0.0 copy-done
  94.2 0.7 copy.22
Async XLA Ops:
  0.6 0.8 copy-start.1
  1.5 0.7 copy-start.4
  2.1 0.7 copy-start.3
  2.8 0.7 copy-start.2
  92.6 1.6 %copy-start = (bf16[128,512]{1,0:T(8,128)(2,1)S(1)}, bf16[128,512]{1,0:T(8,128)(2,1)}, u32[]{:S(2)}) copy-start(bf16[128,512]{1,0:T(8,128)(2,1)} %get-tuple-element.5) | copy-start | bytes 393220

commit v2 on v1

v2 whole, which is shorter than its diff:
```python
import jax
import jax.numpy as jnp
from jax import lax
from jax.experimental import pallas as pl
from jax.experimental.pallas import tpu as pltpu
from jax.sharding import PartitionSpec as P

HD = 64
LOG2E = 1.4426950408889634
ROWS = 128


def dot_rows(a, b):
    return lax.dot_general(a, b, (((1,), (1,)), ((), ())), preferred_element_type=jnp.float32)


def block_update(lhs, off, pairs, tri, near, masks):
    dots = [
        jnp.dot(lhs, jnp.concatenate([kv, kv], axis=0), preferred_element_type=jnp.float32) for kv, _ in pairs
    ]
    logs, sums, heads_of = [], [], []
    for n, (d, (_, bias)) in enumerate(zip(dots, pairs)):
        s = jnp.concatenate(
            [d[h * ROWS : (h + 1) * ROWS] + (bias - off[h]) for h in range(len(off))], axis=0
        )
        soft = jnp.maximum(s, jnp.log2(1.0 + jnp.exp2(jnp.minimum(s, 126.0))))
        logw = s - soft
        if masks is not None:
            row = lax.broadcasted_iota(jnp.int32, s.shape, 0) % ROWS + masks[n]
            later = row > lax.broadcasted_iota(jnp.int32, s.shape, 1)
            soft = jnp.where(later, soft, 0.0)
            logw = jnp.where(later, logw, -jnp.inf)
        logs.append(logw)
        heads_of.append(soft[:, :1])
        sums.append(jnp.dot(soft.astype(jnp.bfloat16), tri, preferred_element_type=jnp.float32))
    out = None
    for logw, total, first, (kv, _) in zip(logs, sums, heads_of, pairs):
        value = dot_rows(jnp.exp2(logw - total).astype(jnp.bfloat16), kv)
        if near is not None:
            value = value * jnp.exp2(-near)
        out = value if out is None else out + value
        step = jnp.broadcast_to(total[:, :1] + first, (total.shape[0], ROWS))
        near = step if near is None else near + step
    return out, near


def query_lhs(q):
    q2 = q.astype(jnp.float32) * (0.125 * LOG2E)
    hi = q2.astype(jnp.bfloat16)
    lo = (q2 - hi.astype(jnp.float32)).astype(jnp.bfloat16)
    zero = jnp.zeros((ROWS, HD), jnp.bfloat16)
    parts = []
    for h in range(q.shape[1] // HD):
        cut = slice(h * HD, (h + 1) * HD)
        parts.append(jnp.concatenate([hi[:, cut], zero, lo[:, cut], zero], axis=1))
    return jnp.concatenate(parts, axis=0)


def triangle():
    r = lax.broadcasted_iota(jnp.int32, (2 * ROWS, 2 * ROWS), 0)
    c = lax.broadcasted_iota(jnp.int32, (2 * ROWS, 2 * ROWS), 1)
    return jnp.where(r > c, 1.0, 0.0).astype(jnp.bfloat16)


NX, NC, CAP = 4, 2, 8
DISTANCES = ((0,), (2, 6), (3, 5, 4), (1, 7))
MESH = pl.DeviceIdType.MESH


def whole_kernel(
    off_ref, kt_ref, vt_ref, bias_ref, q_ref, act_ref, gain_ref, idxt_ref, routet_ref, wg_hbm, wu_hbm, wd_hbm, wo_hbm,
    att_out, exp_out,
    kvb, lhs_ref, tri_ref, acc_ref, near_ref, qfar, far, landed, attended_ref,
    wg, wu, wd, wo,
    outgoing, pick, scale, direct, arr, hid, res, ret,
    apart, aland,
    wsem, lsem, kzs, kzr, kxs, kxr, kcs, kcr, ds, dr, ags, agr, hgs, hgr, wds, wdr, rts, rtr, ats, atr, qss, qsr,
):
    e, t = lax.axis_index("ep"), lax.axis_index("tp")
    nz = lax.axis_size("ep") // (NX * NC)
    ne = nz * NX * NC
    tokens = act_ref.shape[0]
    heads = q_ref.shape[1] // HD
    groups = len(DISTANCES)
    count = [len(d) * NX * NC for d in DISTANCES]
    wide = arr.shape[-1]
    z, x, c = e // (NX * NC), e // NC % NX, e % NC
    xc = x * NC + c
    left, right, opp = (t + 3) % 4, (t + 1) % 4, (t + 2) % 4

    def ep_of(z_, x_, c_):
        return (z_ * NX + x_) * NC + c_

    def rc(src, dst, ssem, rsem, dev):
        return pltpu.make_async_remote_copy(
            src_ref=src, dst_ref=dst, send_sem=ssem, recv_sem=rsem, device_id=dev, device_id_type=MESH
        )

    barrier = pltpu.get_barrier_semaphore()

    def greet(i, carry):
        pl.semaphore_signal(barrier, inc=1, device_id=((e + i) % ne, t), device_id_type=MESH)
        return carry

    lax.fori_loop(1, ne, greet, 0)
    for near_t in (left, right, opp):
        pl.semaphore_signal(barrier, inc=1, device_id=(e, near_t), device_id_type=MESH)

    ff = wd_hbm.shape[0]

    def columns(to):
        return wd_hbm.at[:, pl.ds(pl.multiple_of(to * wide, wide), wide)]

    def part_rows(of):
        return wd.at[pl.ds(pl.multiple_of(of * ff, ff), ff)]

    loads = [
        pltpu.make_async_copy(src, dst, wsem.at[i])
        for i, (src, dst) in enumerate(((wg_hbm, wg), (wu_hbm, wu), (columns(t), part_rows(t)), (wo_hbm, wo)))
    ]
    for load in loads:
        load.start()
    kvb[xc, z] = jnp.concatenate(
        [kt_ref[...], vt_ref[...], jnp.broadcast_to(bias_ref[...].astype(jnp.float32), (16, ROWS)).astype(jnp.bfloat16)],
        axis=0,
    )

    pl.semaphore_wait(barrier, ne + 2)

    zr, zl = (ep_of((z + 1) % nz, x, c), t), (ep_of((z + nz - 1) % nz, x, c), t)

    def round_z(way, step):
        if way == 0:
            i, dev = (z + nz - step) % nz, zr
        else:
            i, dev = (z + step) % nz, zl
        return rc(kvb.at[xc, i], kvb.at[xc, i], kzs.at[way, step], kzr.at[way, step], dev)

    steps_z = (nz // 2, nz - 1 - nz // 2)
    kz = [[round_z(way, step) for step in range(steps_z[way])] for way in range(2)]

    def kv_round(step):
        for way in range(2):
            if 0 < step <= steps_z[way]:
                kz[way][step - 1].wait_recv()
            if step < steps_z[way]:
                kz[way][step].start()

    kv_round(0)

    at_right, at_left = (e, right), (e, left)
    wsend = [
        rc(columns(to), part_rows(t), wds.at[i], wdr.at[i], (e, to)) for i, to in enumerate((right, left, opp))
    ]

    def weights_ready():
        for copy in wsend:
            copy.wait_recv()
        for load in loads[2:]:
            load.wait()

    def loads_ready():
        for load in loads[:2]:
            load.wait()

    for copy in wsend:
        copy.start()

    values = act_ref[...].astype(jnp.float32)
    inv = lax.rsqrt(jnp.mean(values * values, axis=1, keepdims=True) + 1e-06)
    mine = pl.ds(pl.multiple_of(t * wide, wide), wide)
    i0 = lax.broadcasted_iota(jnp.int32, (tokens, tokens), 0)
    i1 = lax.broadcasted_iota(jnp.int32, (tokens, tokens), 1)
    below = jnp.where(i0 > i1, 1.0, 0.0).astype(jnp.bfloat16)
    above = jnp.where(i0 < i1, 1.0, 0.0).astype(jnp.bfloat16)
    idxt = [idxt_ref[k : k + 1, :] for k in range(2)]
    index = jnp.concatenate([idxt_ref[...].astype(jnp.float32), routet_ref[...], jnp.zeros((tokens - 4, tokens), jnp.float32)], axis=0).T
    scale[...] = index
    eq = [jnp.where(i1.astype(jnp.float32) == index[:, k : k + 1], 1.0, 0.0) for k in range(2)]
    prefix = jnp.dot(below, (eq[0] + eq[1]).astype(jnp.bfloat16), preferred_element_type=jnp.float32)
    eqt = [jnp.where(i0 == idxt[k], 1.0, 0.0) for k in range(2)]
    prefixt = jnp.dot((eqt[0] + eqt[1]).astype(jnp.bfloat16), above, preferred_element_type=jnp.float32)
    slots = ne * CAP
    col = lax.broadcasted_iota(jnp.int32, (tokens, slots), 1).astype(jnp.float32)
    row = lax.broadcasted_iota(jnp.int32, (slots, tokens), 0).astype(jnp.float32)
    spread = None
    for k in range(2):
        place = jnp.sum(eq[k] * prefix, axis=1, keepdims=True) + index[:, k : k + 1] * CAP
        pick[k] = jnp.where(col == place, 1.0, 0.0).astype(jnp.bfloat16)
        placet = jnp.sum(eqt[k] * prefixt, axis=0, keepdims=True) + idxt[k].astype(jnp.float32) * CAP
        one = jnp.where(row == placet, 1.0, 0.0)
        spread = one if spread is None else spread + one
    spread = spread.astype(jnp.bfloat16)
    for s in range(0, act_ref.shape[1], wide):
        cols = slice(s, s + wide)
        normed = (act_ref[:, cols].astype(jnp.float32) * inv * gain_ref[:, cols]).astype(jnp.bfloat16)
        sent = jnp.dot(spread, normed, preferred_element_type=jnp.float32)
        outgoing[:, :, cols] = sent.reshape(ne, CAP, wide).astype(jnp.bfloat16)
    lhs_ref[0] = query_lhs(q_ref[...])
    acc_ref[1] = jnp.zeros(acc_ref.shape[1:], jnp.float32)
    near_ref[1] = jnp.zeros(near_ref.shape[1:], jnp.float32)
    tri_ref[...] = triangle()
    off = [off_ref[h] * LOG2E for h in range(heads)]

    def peer(g, i, sign):
        per = NX * NC
        dz = DISTANCES[g][-1] % nz
        for n in range(len(DISTANCES[g]) - 1, 0, -1):
            dz = jnp.where(i < n * per, DISTANCES[g][n - 1] % nz, dz)
        dx, dc = i // NC % NX, i % NC
        if sign < 0:
            dz, dx = nz - dz, NX - dx
        return ep_of((z + dz) % nz, (x + dx) % NX, (c + dc) % NC)

    own_rows = pltpu.make_async_copy(outgoing.at[e], direct.at[0], lsem.at[1])
    own_rows.start()
    def dispatch(g, first=0, last=3):
        def scatter(i, carry):
            to = peer(g, i, 1)
            if g == 0:
                src, dst = outgoing.at[to], direct.at[i]
            else:
                src, dst = outgoing.at[to, :, mine], arr.at[t, g - 1, i]
            rc(src, dst, ds.at[g], dr.at[g], (to, t)).start()
            return carry

        per = NX * NC
        lax.fori_loop(1 if g == 0 else first * per, min(last * per, count[g]), scatter, 0)

    def arrived(g):
        ref = direct.at[1:] if g == 0 else arr.at[t, g - 1, : count[g]]
        return rc(ref, ref, ds.at[g], dr.at[g], (e, t))

    def ag(g):
        n, half = count[g], count[g] // 2
        a, left_rows, right_rows = arr.at[t, g - 1, :n], arr.at[left, g - 1, :half], arr.at[right, g - 1, half:n]
        return [
            rc(a, a, ags.at[0, g], agr.at[0, g], at_right),
            rc(a, a, ags.at[1, g], agr.at[1, g], at_left),
            rc(left_rows, left_rows, ags.at[2, g], agr.at[2, g], at_right),
            rc(right_rows, right_rows, ags.at[3, g], agr.at[3, g], at_left),
        ]

    ags_all = [[]] + [ag(g) for g in range(1, groups)]

    def spread_rows(g):
        arrived(g).wait_recv()
        ags_all[g][0].start()
        ags_all[g][1].start()

    def forward_rows(g):
        ags_all[g][0].wait_recv()
        ags_all[g][2].start()
        ags_all[g][1].wait_recv()
        ags_all[g][3].start()

    xl, xr, xo = (x + 3) % NX, (x + 1) % NX, (x + 2) % NX
    dev_xr, dev_xl, dev_c = (ep_of(z, xr, c), t), (ep_of(z, xl, c), t), (ep_of(z, x, (c + 1) % NC), t)
    zh = nz // 2

    def grp(x_):
        return kvb.at[x_ * NC + c]

    kx = [
        rc(grp(x), grp(x), kxs.at[0], kxr.at[0], dev_xr),
        rc(grp(x), grp(x), kxs.at[1], kxr.at[1], dev_xl),
        rc(kvb.at[xl * NC + c, :zh], kvb.at[xl * NC + c, :zh], kxs.at[2], kxr.at[2], dev_xr),
        rc(kvb.at[xr * NC + c, zh:], kvb.at[xr * NC + c, zh:], kxs.at[3], kxr.at[3], dev_xl),
    ]
    kc = [rc(grp(x_), grp(x_), kcs.at[i], kcr.at[i], dev_c) for i, x_ in enumerate((x, xl, xr, xo))]

    def kv_first():
        kv_round(4)
        kx[0].start()
        kx[1].start()
        kc[0].start()

    def kv_second():
        kx[0].wait_recv()
        kx[2].start()
        kc[1].start()
        kx[1].wait_recv()
        kx[3].start()
        kc[2].start()

    def kv_third():
        kx[2].wait_recv()
        kx[3].wait_recv()
        kc[3].start()

    def kv_ready():
        for copy in kc:
            copy.wait_recv()


    def flat(ref):
        v = ref[...].astype(jnp.float32)
        return v.reshape(v.shape[0] * v.shape[1], v.shape[2])

    def experts(g):
        if g == 0:
            arrived(0).wait_recv()
            own_rows.wait()
            xs = flat(direct).astype(jnp.bfloat16)
        else:
            ags_all[g][2].wait_recv()
            ags_all[g][3].wait_recv()
            xs = jnp.concatenate([flat(arr.at[s, g - 1, : count[g]]).astype(jnp.bfloat16) for s in range(4)], axis=1)
        gate = jnp.dot(xs, wg[...], preferred_element_type=jnp.float32)
        up = jnp.dot(xs, wu[...], preferred_element_type=jnp.float32)
        hidden = (gate / (1.0 + jnp.exp(-gate)) * up).astype(jnp.bfloat16)
        hid[t, g, : count[g] * CAP] = hidden
        hgs_all[g][0].start()
        hgs_all[g][1].start()

    def hg(g):
        rows, half = count[g] * CAP, count[g] * CAP // 2
        a, left_rows, right_rows = hid.at[t, g, :rows], hid.at[left, g, :half], hid.at[right, g, half:rows]
        return [
            rc(a, a, hgs.at[0, g], hgr.at[0, g], at_right),
            rc(a, a, hgs.at[1, g], hgr.at[1, g], at_left),
            rc(left_rows, left_rows, hgs.at[2, g], hgr.at[2, g], at_right),
            rc(right_rows, right_rows, hgs.at[3, g], hgr.at[3, g], at_left),
        ]

    hgs_all = [hg(g) for g in range(groups)]

    def forward_hidden(g):
        hgs_all[g][0].wait_recv()
        hgs_all[g][2].start()
        hgs_all[g][1].wait_recv()
        hgs_all[g][3].start()

    own_back = pltpu.make_async_copy(res.at[0, 0], ret.at[e], lsem.at[2])

    def give_back(g):
        hgs_all[g][2].wait_recv()
        hgs_all[g][3].wait_recv()
        hidden = jnp.concatenate([hid[s, g, : count[g] * CAP] for s in range(4)], axis=1)
        value = jnp.dot(hidden, wd[...], preferred_element_type=jnp.float32)
        res[g, : count[g]] = value.reshape(count[g], CAP, wide).astype(jnp.bfloat16)
        if g == 0:
            own_back.start()

        def back(i, carry):
            to = peer(g, i, -1)
            rc(res.at[g, i], ret.at[e], rts.at[g], rtr, (to, t)).start()
            return carry

        lax.fori_loop(1 if g == 0 else 0, count[g], back, 0)

    def load_pair(b):
        i, j = b % (NX * NC), b // (NX * NC)
        kv = jnp.concatenate([kvb[i, j, :ROWS], kvb[i + 1, j, :ROWS]], axis=1)
        bias = jnp.concatenate([kvb[i, j, ROWS:][:1], kvb[i + 1, j, ROWS:][:1]], axis=1)
        return kv, bias.astype(jnp.float32) * LOG2E

    heavy, light = z >= nz // 2, z < nz // 2
    shared = jnp.where(heavy, 2 * z + 1 - nz, nz - 1 - 2 * z) * (NX * NC // 8)
    partner = (ep_of(nz - 1 - z, x, c), t)
    ask = rc(q_ref, qfar, qss.at[0], qsr.at[0], partner)
    answer = rc(far, landed, qss.at[1], qsr.at[1], partner)

    def attend_quad(slot, quad, first):
        pairs = [load_pair(quad * 4 + 2), load_pair(quad * 4)]
        own = e % 4 * ROWS
        lhs, tri = lhs_ref[slot], tri_ref[...]
        near = None if first else near_ref[slot]
        result = block_update(lhs, off, pairs, tri, near, (own - 2 * ROWS, own) if first else None)
        acc_ref[slot] = result[0] if first else acc_ref[slot] + result[0]
        near_ref[slot] = result[1]

    def packed(ref):
        lane = lax.broadcasted_iota(jnp.int32, (ROWS, ROWS), 1)
        pairs = []
        for h in range(0, heads, 2):
            even = pltpu.roll(ref[h * ROWS : (h + 1) * ROWS, :], HD, 1)
            odd = ref[(h + 1) * ROWS : (h + 2) * ROWS, :]
            pairs.append(jnp.where(lane < HD, even, odd))
        return jnp.concatenate(pairs, axis=1)

    def ask_partner():
        @pl.when(heavy)
        def _():
            ask.start()

    def attend_far_start():
        @pl.when(light)
        def _():
            ask.wait_recv()
            lhs_ref[1] = query_lhs(qfar[...])

    def attend_far(piece, pieces):
        much = jnp.where(light, shared, 0)

        def step(i, carry):
            attend_quad(1, much - 1 - i, False)
            return carry

        lax.fori_loop(much * piece // pieces, much * (piece + 1) // pieces, step, 0)

    def attend_far_send():
        @pl.when(light)
        def _():
            far[...] = packed(acc_ref.at[1]).astype(jnp.bfloat16)
            answer.start()

    quads = e // 4

    def attend_first():
        attend_quad(0, quads, True)

    def attend(piece, pieces):
        much = quads - jnp.where(heavy, shared, 0)

        def step(i, carry):
            attend_quad(0, quads - i, False)
            return carry

        lax.fori_loop(1 + much * piece // pieces, 1 + much * (piece + 1) // pieces, step, 0)

    aw = apart.shape[1]
    ar = [
        rc(apart.at[to], aland.at[i], ats.at[i], atr.at[i], (e, to)) for i, to in enumerate((right, left, opp))
    ]

    def project():
        attended_ref[...] = packed(acc_ref.at[0])

        @pl.when(heavy)
        def _():
            answer.wait_recv()
            attended_ref[...] += jnp.exp2(-packed(near_ref.at[0])) * landed[...].astype(jnp.float32)

        attended = attended_ref[...].astype(jnp.bfloat16)
        step = 512
        for s in range(0, wo.shape[1], step):
            value = jnp.dot(attended, wo[:, s : s + step], preferred_element_type=jnp.float32)
            apart[:, :, s : s + step] = value.reshape(4, aw, step).astype(jnp.bfloat16)
        for copy in ar:
            copy.start()

    def project_last():
        total = apart[t].astype(jnp.float32)
        for i, copy in enumerate(ar):
            copy.wait_recv()
            total = total + aland[i].astype(jnp.float32)
        att_out[...] = total.astype(jnp.bfloat16)

    def finish():
        all_back = rc(ret.at[1:], ret.at[1:], rts.at[0], rtr, (e, t))
        all_back.wait_recv()
        own_back.wait()
        back_rows = flat(ret).astype(jnp.bfloat16)
        total = None
        for k in range(2):
            got = jnp.dot(pick[k], back_rows, preferred_element_type=jnp.float32) * scale[:, 2 + k : 3 + k]
            total = got if total is None else total + got
        exp_out[...] = total.astype(jnp.bfloat16)
        project_last()

    dispatch(1)
    kv_round(1)
    dispatch(2, 0, 2)
    kv_round(2)
    dispatch(2, 2, 3)
    ask_partner()
    spread_rows(1)
    kv_round(3)
    dispatch(3)
    forward_rows(1)
    kv_first()
    dispatch(0)
    spread_rows(2)
    loads_ready()
    spread_rows(3)
    experts(1)
    forward_rows(2)
    kv_second()
    experts(0)
    weights_ready()
    forward_hidden(1)
    forward_rows(3)
    kv_third()
    experts(2)
    give_back(1)
    forward_hidden(0)
    kv_ready()
    attend_far_start()
    attend_far(0, 2)
    experts(3)
    forward_hidden(2)
    give_back(0)
    attend_far(1, 2)
    attend_far_send()
    attend_first()
    attend(0, 4)
    forward_hidden(3)
    give_back(2)
    attend(1, 4)
    attend(2, 4)
    give_back(3)
    attend(3, 4)
    project()
    finish()

    for g in range(groups):
        arrived(g).wait_send()
        ref = res.at[g, 1 if g == 0 else 0 : count[g]]
        rc(ref, ref, rts.at[g], rtr, (e, t)).wait_send()
        for copy in ags_all[g] + hgs_all[g]:
            copy.wait_send()
    @pl.when(heavy)
    def _():
        ask.wait_send()

    @pl.when(light)
    def _():
        answer.wait_send()

    for copy in kz[0] + kz[1] + kx + kc + ar + wsend:
        copy.wait_send()


def body(
    query_rows, key_rows, retrieved_vector_table, key_bias, score_offset, out_weight, second_batch_activations,
    norm_gain, expert_index, route_weight, gate_weight, up_weight, down_weight,
):
    ne = lax.axis_size("ep")
    tokens, width = second_batch_activations.shape
    wide = width // 4
    groups = len(DISTANCES)
    most = max(len(d) for d in DISTANCES) * NX * NC
    many = max(len(d) for d in DISTANCES[1:]) * NX * NC
    heads = query_rows.shape[1] // HD
    bf, f32 = jnp.bfloat16, jnp.float32
    vmem, dma = pltpu.VMEM, pltpu.SemaphoreType.DMA
    vspec, aspec = pl.BlockSpec(memory_space=pltpu.VMEM), pl.BlockSpec(memory_space=pl.ANY)
    aw = tokens // 4
    return pl.pallas_call(
        whole_kernel,
        out_shape=(
            jax.ShapeDtypeStruct((aw, width), bf),
            jax.ShapeDtypeStruct((tokens, wide), bf),
        ),
        in_specs=[pl.BlockSpec(memory_space=pltpu.SMEM)] + [vspec] * 8 + [aspec] * 4,
        out_specs=(vspec, vspec),
        scratch_shapes=[
            vmem((NX * NC, ne // (NX * NC), ROWS + 16, ROWS), bf),
            vmem((2, heads * ROWS, 2 * ROWS), bf),
            vmem((2 * ROWS, 2 * ROWS), bf),
            vmem((2, heads * ROWS, ROWS), f32),
            vmem((2, heads * ROWS, ROWS), f32),
            vmem((ROWS, heads * HD), bf),
            vmem((ROWS, heads * HD), bf),
            vmem((ROWS, heads * HD), bf),
            vmem((ROWS, heads * HD), f32),
            vmem(gate_weight.shape[1:], bf),
            vmem(up_weight.shape[1:], bf),
            vmem((4 * down_weight.shape[1], wide), bf),
            vmem(out_weight.shape, bf),
            vmem((ne, CAP, width), bf),
            vmem((2, tokens, ne * CAP), bf),
            vmem((tokens, tokens), f32),
            vmem((len(DISTANCES[0]) * NX * NC, CAP, width), bf),
            vmem((4, groups - 1, many, CAP, wide), bf),
            vmem((4, groups, most * CAP, gate_weight.shape[2]), bf),
            vmem((groups, most, CAP, wide), bf),
            vmem((ne, CAP, wide), bf),
            vmem((4, aw, width), bf),
            vmem((3, aw, width), bf),
            dma((4,)), dma((3,)), dma((2, 4)), dma((2, 4)), dma((4,)), dma((4,)), dma((4,)), dma((4,)),
            dma((groups,)), dma((groups,)), dma((4, groups)), dma((4, groups)), dma((4, groups)), dma((4, groups)), dma((3,)), dma((3,)),
            dma((groups,)), dma, dma((3,)), dma((3,)), dma((2,)), dma((2,)),
        ],
        compiler_params=pltpu.CompilerParams(
            collective_id=0, has_side_effects=True, vmem_limit_bytes=56 * 1024 * 1024
        ),
    )(
        score_offset, key_rows.T, retrieved_vector_table.T, key_bias.T, query_rows, second_batch_activations,
        norm_gain.reshape(1, width), expert_index.T, route_weight.T, gate_weight[0], up_weight[0], down_weight[0],
        out_weight,
    )


def solution(mesh):
    return jax.shard_map(
        body,
        mesh=mesh,
        in_specs=(
            P("ep", "tp"),
            P("ep", "tp"),
            P("ep", "tp"),
            P("ep", "tp"),
            P("tp"),
            P("tp", None),
            P("ep", None),
            P(),
            P("ep", None),
            P("ep", None),
            P("ep", None, "tp"),
            P("ep", None, "tp"),
            P("ep", "tp", None),
        ),
        out_specs=(P(("ep", "tp"), None), P("ep", "tp")),
        check_vma=False,
    )
```

time: 95.1 us -> 73.6 us (0.77)
  the two profiles are of different devices: /device:TPU:64 before, /device:TPU:1 now
where the time goes in v2:
time: 73.6 us; the launch traced here: 73.5 us
  Pallas kernels  70.6 us (96%)
  local copies, waits for them, and re-layouts  2.26 us (3%)
    pallas_call x1, Pallas kernels, body(): pl.pallas_call(whole_kernel, out_shape=(jax.ShapeDtypeStruct((aw, width),...  70.6 us
    unnamed x4, local copies, waits for them, and re-layouts  2.26 us

profile of v2, /device:TPU:1, one launch (start us, length us, event | category | flops | bytes accessed | tf_op | source)
XLA Modules:
  0.0 73.5 jit_solution(15948941135608206878)
XLA Ops:
  0.6 70.6 %shard_map.140 = (bf16[32,2048]{1,0:T(8,128)(2,1)}, bf16[128,512]{1,0:T(8,128)(2,1)}) custom-call(f32[4]{0:T(128)} %off_ref.1, bf16[64,128]{1,0:T(8,128)(2,1)} %bitcast.12, bf16[64,128]{1,0:T(8,128)(2,1)} %bitcast.13, bf16[1,128]{1,0:T(2,128)(2,1)} %bitcast.17, bf16[128,256]{1,0:T(8,128)(2,1)} %q_ref.1, bf16[128,2048]{1,0:T(8,128)(2,1)} %act_ref.1, ...), custom_call_target="tpu_custom_call" | custom-call | tf_op jit(solution)/shard_map/pallas_call | solution.py:540
  71.2 0.0 copy-start
  71.2 1.6 %copy.17 = bf16[32,2048]{1,0:T(8,128)(2,1)} copy(bf16[32,2048]{1,0:T(8,128)(2,1)} %get-tuple-element.4) | data formatting | bytes 262144
  72.8 0.0 copy-done
  72.8 0.7 copy.18
Async XLA Ops:
  71.2 1.6 %copy-start = (bf16[128,512]{1,0:T(8,128)(2,1)S(1)}, bf16[128,512]{1,0:T(8,128)(2,1)}, u32[]{:S(2)}) copy-start(bf16[128,512]{1,0:T(8,128)(2,1)} %get-tuple-element.5) | copy-start | bytes 393220

commit v3 on v2

--- a/solution.py
+++ b/solution.py
@@ -63,7 +63,7 @@
 
 
 NX, NC, CAP = 4, 2, 8
-DISTANCES = ((0,), (2, 6), (3, 5, 4), (1, 7))
+DISTANCES = ((0,), (3, 5, 4), (2, 6), (1, 7))
 MESH = pl.DeviceIdType.MESH
 
 
@@ -410,14 +410,15 @@
     def attend_first():
         attend_quad(0, quads, True)
 
-    def attend(piece, pieces):
+    def attend(late, early, pieces):
         much = quads - jnp.where(heavy, shared, 0)
+        lo, hi = jnp.where(heavy, late[0], early[0]), jnp.where(heavy, late[1], early[1])
 
         def step(i, carry):
             attend_quad(0, quads - i, False)
             return carry
 
-        lax.fori_loop(1 + much * piece // pieces, 1 + much * (piece + 1) // pieces, step, 0)
+        lax.fori_loop(1 + much * lo // pieces, 1 + much * hi // pieces, step, 0)
 
     aw = apart.shape[1]
     ar = [
@@ -447,62 +448,65 @@
             total = total + aland[i].astype(jnp.float32)
         att_out[...] = total.astype(jnp.bfloat16)
 
-    def finish():
+    def returned():
         all_back = rc(ret.at[1:], ret.at[1:], rts.at[0], rtr, (e, t))
         all_back.wait_recv()
         own_back.wait()
+
+    def combine():
         back_rows = flat(ret).astype(jnp.bfloat16)
         total = None
         for k in range(2):
             got = jnp.dot(pick[k], back_rows, preferred_element_type=jnp.float32) * scale[:, 2 + k : 3 + k]
             total = got if total is None else total + got
         exp_out[...] = total.astype(jnp.bfloat16)
-        project_last()
-
-    dispatch(1)
+
+    dispatch(1, 0, 2)
     kv_round(1)
-    dispatch(2, 0, 2)
+    dispatch(1, 2, 3)
     kv_round(2)
-    dispatch(2, 2, 3)
+    dispatch(2)
+    dispatch(0)
+    kv_round(3)
+    spread_rows(1)
+    dispatch(3)
     ask_partner()
-    spread_rows(1)
-    kv_round(3)
-    dispatch(3)
+    kv_first()
+    spread_rows(2)
     forward_rows(1)
-    kv_first()
-    dispatch(0)
-    spread_rows(2)
     loads_ready()
+    experts(0)
     spread_rows(3)
+    kv_second()
     experts(1)
     forward_rows(2)
-    kv_second()
-    experts(0)
+    forward_hidden(0)
+    kv_third()
     weights_ready()
-    forward_hidden(1)
     forward_rows(3)
-    kv_third()
-    experts(2)
-    give_back(1)
-    forward_hidden(0)
     kv_ready()
     attend_far_start()
     attend_far(0, 2)
-    experts(3)
-    forward_hidden(2)
-    give_back(0)
+    attend_first()
+    forward_hidden(1)
+    attend((0, 1), (0, 0), 4)
+    experts(2)
     attend_far(1, 2)
     attend_far_send()
-    attend_first()
-    attend(0, 4)
+    attend((1, 2), (0, 0), 4)
+    give_back(1)
+    experts(3)
+    give_back(0)
+    forward_hidden(2)
+    attend((2, 3), (0, 1), 4)
     forward_hidden(3)
     give_back(2)
-    attend(1, 4)
-    attend(2, 4)
+    attend((3, 4), (1, 4), 4)
     give_back(3)
-    attend(3, 4)
     project()
-    finish()
+    returned()
+    combine()
+    project_last()
 
     for g in range(groups):
         arrived(g).wait_send()

time: 73.6 us -> 72.4 us (0.984)
  Pallas kernels: 70.6 us -> 69.4 us
    pallas_call x1, Pallas kernels: 70.6 us -> 69.4 us  [body(): pl.pallas_call(whole_kernel, out_shape=(jax.ShapeDtypeStruct((aw, width),...]
where the time goes in v3:
time: 72.4 us; the launch traced here: 72.3 us
  Pallas kernels  69.4 us (96%)
  local copies, waits for them, and re-layouts  2.26 us (3%)
    pallas_call x1, Pallas kernels, body(): pl.pallas_call(whole_kernel, out_shape=(jax.ShapeDtypeStruct((aw, width),...  69.4 us
    unnamed x4, local copies, waits for them, and re-layouts  2.26 us

profile of v3, /device:TPU:1, one launch (start us, length us, event | category | flops | bytes accessed | tf_op | source)
XLA Modules:
  0.0 72.3 jit_solution(13850191474645634362)
XLA Ops:
  0.6 69.4 %shard_map.140 = (bf16[32,2048]{1,0:T(8,128)(2,1)}, bf16[128,512]{1,0:T(8,128)(2,1)}) custom-call(f32[4]{0:T(128)} %off_ref.1, bf16[64,128]{1,0:T(8,128)(2,1)} %bitcast.12, bf16[64,128]{1,0:T(8,128)(2,1)} %bitcast.13, bf16[1,128]{1,0:T(2,128)(2,1)} %bitcast.17, bf16[128,256]{1,0:T(8,128)(2,1)} %q_ref.1, bf16[128,2048]{1,0:T(8,128)(2,1)} %act_ref.1, ...), custom_call_target="tpu_custom_call" | custom-call | tf_op jit(solution)/shard_map/pallas_call | solution.py:544
  70.0 0.0 copy-start
  70.0 1.6 %copy.17 = bf16[32,2048]{1,0:T(8,128)(2,1)} copy(bf16[32,2048]{1,0:T(8,128)(2,1)} %get-tuple-element.4) | data formatting | bytes 262144
  71.6 0.0 copy-done
  71.6 0.7 copy.18
Async XLA Ops:
  70.0 1.6 %copy-start = (bf16[128,512]{1,0:T(8,128)(2,1)S(1)}, bf16[128,512]{1,0:T(8,128)(2,1)}, u32[]{:S(2)}) copy-start(bf16[128,512]{1,0:T(8,128)(2,1)} %get-tuple-element.5) | copy-start | bytes 393220

commit v4 on v3

--- a/solution.py
+++ b/solution.py
@@ -102,7 +102,7 @@
         pl.semaphore_signal(barrier, inc=1, device_id=((e + i) % ne, t), device_id_type=MESH)
         return carry
 
-    lax.fori_loop(1, ne, greet, 0)
+    lax.fori_loop(1, ne, greet, 0, unroll=True)
     for near_t in (left, right, opp):
         pl.semaphore_signal(barrier, inc=1, device_id=(e, near_t), device_id_type=MESH)
 

time: 72.4 us -> 72.2 us (level)
  no operation moved by 1% of the time
where the time goes in v4:
time: 72.2 us; the launch traced here: 72.1 us
  Pallas kernels  69.1 us (96%)
  local copies, waits for them, and re-layouts  2.26 us (3%)
    pallas_call x1, Pallas kernels, body(): pl.pallas_call(whole_kernel, out_shape=(jax.ShapeDtypeStruct((aw, width),...  69.1 us
    unnamed x4, local copies, waits for them, and re-layouts  2.26 us

profile of v4, /device:TPU:1, one launch (start us, length us, event | category | flops | bytes accessed | tf_op | source)
XLA Modules:
  0.0 72.1 jit_solution(14646035509775022699)
XLA Ops:
  0.6 69.1 %shard_map.140 = (bf16[32,2048]{1,0:T(8,128)(2,1)}, bf16[128,512]{1,0:T(8,128)(2,1)}) custom-call(f32[4]{0:T(128)} %off_ref.1, bf16[64,128]{1,0:T(8,128)(2,1)} %bitcast.12, bf16[64,128]{1,0:T(8,128)(2,1)} %bitcast.13, bf16[1,128]{1,0:T(2,128)(2,1)} %bitcast.17, bf16[128,256]{1,0:T(8,128)(2,1)} %q_ref.1, bf16[128,2048]{1,0:T(8,128)(2,1)} %act_ref.1, ...), custom_call_target="tpu_custom_call" | custom-call | tf_op jit(solution)/shard_map/pallas_call | solution.py:544
  69.8 0.0 copy-start
  69.8 1.6 %copy.17 = bf16[32,2048]{1,0:T(8,128)(2,1)} copy(bf16[32,2048]{1,0:T(8,128)(2,1)} %get-tuple-element.4) | data formatting | bytes 262144
  71.4 0.0 copy-done
  71.4 0.7 copy.18
Async XLA Ops:
  69.8 1.6 %copy-start = (bf16[128,512]{1,0:T(8,128)(2,1)S(1)}, bf16[128,512]{1,0:T(8,128)(2,1)}, u32[]{:S(2)}) copy-start(bf16[128,512]{1,0:T(8,128)(2,1)} %get-tuple-element.5) | copy-start | bytes 393220
